TPU v7x, 32 devices: a whole 2x2x4 slice. The times are simulated.
32 devices in a mesh: grp: 2 (over y), ra: 4 (over z), cb: 4 (over x, core).
Axes of the slice: x: 2, y: 2, z: 4, core: 2. Of those that a mesh axis runs over, the one named last changes fastest.
Arguments:
- tokens: bfloat16 [512, 4096], P('grp', 'cb'), parts along dimension 0, may hold values from -50 to 50
- norm_gains: float32 [3, 4096], P(None, 'cb'), may hold values from 0.1 to 1.9
- gate_weight: float32 [2, 4096, 11264], P(None, 'cb', 'ra'), may hold values from -0.09375 to 0.09375
- value_weight: float32 [2, 4096, 11264], P(None, 'cb', 'ra'), may hold values from -0.09375 to 0.09375
- gate_scale: float32 [2, 11264], P(None, 'ra'), may hold values from 0.3 to 3
- value_scale: float32 [2, 11264], P(None, 'ra'), may hold values from 0.3 to 3
- conv_gate: float32 [2, 3, 11264], P(None, None, 'ra'), may hold values from -3 to 3
- conv_value: float32 [2, 3, 11264], P(None, None, 'ra'), may hold values from -3 to 3
- down_weight: float32 [2, 11264, 4096], P(None, 'ra', 'cb'), may hold values from -0.07537784 to 0.07537784
- down_scale: float32 [2, 4096], P(None, 'cb'), may hold values from 0.3 to 3
Outputs:
- normed_out: bfloat16 [512, 4096], P('grp', 'cb'), parts along dimension 0
There are 2 independent parts, one for each index of `grp`. A program takes and returns all parts, laid end to end along the dimension named above; an argument that names none is the same for every part. Nothing has to cross between parts.
All inputs are finite; a program needn't handle non-finite values.
Results may differ from a plain program's by a relative error of at most 0.012.
The roundings to bfloat16 on the way count: a program that leaves them out, or rounds other values in their place, can miss the bound.
Values may be sent and summed in bfloat16 or wider, within the bound.
A program may use at most 192 MiB of HBM per device.

v0:
```python
import jax
import jax.numpy as jnp
from jax import lax
from jax.sharding import PartitionSpec as P

epsilon = 1e-06
residual_weight = 0.5


def causal_taps(projected, tap_weights):
    tap_count = tap_weights.shape[0]
    row_count = projected.shape[0]
    padded = jnp.pad(projected, ((tap_count - 1, 0), (0, 0)))
    result = jnp.zeros_like(projected)
    for tap_idx in range(tap_count):
        result = result + padded[tap_idx : tap_idx + row_count] * tap_weights[tap_idx]
    return result


def row_inverse(state_wide, model_width):
    squares = lax.psum(jnp.sum(state_wide * state_wide, axis=1, keepdims=True), "cb")
    return lax.rsqrt(squares / model_width + epsilon)


def on_device(
    tokens,
    norm_gains,
    gate_weight,
    value_weight,
    gate_scale,
    value_scale,
    conv_gate,
    conv_value,
    down_weight,
    down_scale,
):
    model_width = lax.axis_size("cb") * tokens.shape[1]
    layer_count = gate_weight.shape[0]
    current = tokens
    for layer_idx in range(layer_count):
        state_wide = current.astype(jnp.float32)
        inverse = row_inverse(state_wide, model_width)
        scaled = (state_wide * norm_gains[layer_idx]).astype(jnp.bfloat16)
        gate_part = jnp.dot(
            scaled, gate_weight[layer_idx].astype(jnp.bfloat16), preferred_element_type=jnp.float32
        )
        value_part = jnp.dot(
            scaled, value_weight[layer_idx].astype(jnp.bfloat16), preferred_element_type=jnp.float32
        )
        gate_sum, value_sum = (
            lax.psum_scatter(gate_part, "cb", scatter_dimension=1, tiled=True),
            lax.psum_scatter(value_part, "cb", scatter_dimension=1, tiled=True),
        )
        share_cols = gate_sum.shape[1]
        first_col = lax.axis_index("cb") * share_cols
        gate_cols = lax.dynamic_slice_in_dim(gate_scale[layer_idx], first_col, share_cols, 0)
        value_cols = lax.dynamic_slice_in_dim(value_scale[layer_idx], first_col, share_cols, 0)
        gate_taps = lax.dynamic_slice_in_dim(conv_gate[layer_idx], first_col, share_cols, 1)
        value_taps = lax.dynamic_slice_in_dim(conv_value[layer_idx], first_col, share_cols, 1)
        gate_pre = inverse * gate_cols * gate_sum
        value_pre = inverse * value_cols * value_sum
        hidden = (
            jax.nn.gelu(causal_taps(gate_pre, gate_taps), approximate=True)
            * causal_taps(value_pre, value_taps)
        ).astype(jnp.bfloat16)
        hidden = lax.all_gather(hidden, "cb", axis=1, tiled=True)
        partial_value = jnp.dot(
            hidden, down_weight[layer_idx].astype(jnp.bfloat16), preferred_element_type=jnp.float32
        )
        down_total = lax.psum(partial_value, "ra")
        current = (residual_weight * state_wide + down_scale[layer_idx] * down_total).astype(
            jnp.bfloat16
        )
    state_wide = current.astype(jnp.float32)
    inverse = row_inverse(state_wide, model_width)
    return (state_wide * inverse * norm_gains[layer_count]).astype(jnp.bfloat16)


def solution(mesh):
    in_specs = (
        P("grp", "cb"),
        P(None, "cb"),
        P(None, "cb", "ra"),
        P(None, "cb", "ra"),
        P(None, "ra"),
        P(None, "ra"),
        P(None, None, "ra"),
        P(None, None, "ra"),
        P(None, "ra", "cb"),
        P(None, "cb"),
    )
    out_specs = P("grp", "cb")
    return jax.shard_map(
        on_device, mesh=mesh, in_specs=in_specs, out_specs=out_specs, check_vma=False
    )
```

profile of v0, /device:TPU:0, one launch (start us, length us, event | category | flops | bytes accessed | tf_op | source)
XLA Modules:
  0.0 362.3 jit_solution(13226815253919093914)
XLA Ops:
  7.4 8.6 %convert.12 = bf16[2,1024,2816]{2,1,0:T(8,128)(2,1)S(1)} convert(f32[2,1024,2816]{2,1,0:T(8,128)} %param.12) | non-fusion elementwise | flops 5767168 | bytes 34603008 | tf_op jit(solution)/shard_map/convert.5
  16.0 4.2 %copy-done.1 = bf16[2,1024,2816]{2,1,0:T(8,128)(2,1)} copy-done((bf16[2,1024,2816]{2,1,0:T(8,128)(2,1)}, bf16[2,1024,2816]{2,1,0:T(8,128)(2,1)S(1)}, u32[]{:S(2)}) %copy-start.1) | copy-done | bytes 11534360
  20.2 4.1 %fusion.5 = f32[256,2816]{0,1:T(8,128)} fusion(bf16[2,1024,2816]{2,1,0:T(8,128)(2,1)S(1)} %convert.12, bf16[256,1024]{1,0:T(8,128)(2,1)S(1)} %copy-done.2, f32[1024]{0:T(1024)S(1)} %bitcast.42), kind=kOutput, calls=%fused_computation.11 | convolution fusion | flops 1477181440 | bytes 9179136 | tf_op jit(solution)/shard_map/dot_general | solution.py:44
  24.4 8.6 %convert.13 = bf16[2,1024,2816]{2,1,0:T(8,128)(2,1)S(1)} convert(f32[2,1024,2816]{2,1,0:T(8,128)} %param.13) | non-fusion elementwise | flops 5767168 | bytes 34603008 | tf_op jit(solution)/shard_map/convert.4
  32.9 4.8 %copy-done = bf16[2,1024,2816]{2,1,0:T(8,128)(2,1)} copy-done((bf16[2,1024,2816]{2,1,0:T(8,128)(2,1)}, bf16[2,1024,2816]{2,1,0:T(8,128)(2,1)S(1)}, u32[]{:S(2)}) %copy-start) | copy-done | bytes 11534360
  37.8 4.0 %fusion.4 = f32[256,2816]{0,1:T(8,128)} fusion(bf16[2,1024,2816]{2,1,0:T(8,128)(2,1)S(1)} %convert.13, bf16[256,1024]{1,0:T(8,128)(2,1)S(1)} %copy-done.2, f32[1024]{0:T(1024)S(1)} %bitcast.43), kind=kOutput, calls=%fused_computation.9 | convolution fusion | flops 1477181440 | bytes 9179136 | tf_op jit(solution)/shard_map/dot_general | solution.py:47
  42.2 9.0 %psum.35 = f32[256,1]{0,1:T(1,128)S(1)} all-reduce(f32[256,1]{0,1:T(1,128)S(1)} %bitcast.39), channel_id=1, replica_groups=mesh['grp'=2,'ra'=4,'cb'=4] {'cb'}, use_global_device_ids=true, to_apply=%region_1.0 | all-reduce | flops 256 | bytes 2048 | tf_op jit(solution)/shard_map/psum | solution.py:21
  51.5 12.1 %reduce-scatter.5.cloned.1.call-done = f32[256,704]{0,1:T(8,128)} async-done(((f32[256,2816]{0,1:T(8,128)}), f32[256,704]{0,1:T(8,128)}) %reduce-scatter.5.cloned.1.call-update) | async-done | bytes 720912 | tf_op jit(solution)/shard_map/reduce_scatter | solution.py:51
  63.5 38.8 %reduce-scatter.7.cloned.1.call-done = f32[256,704]{0,1:T(8,128)} async-done(((f32[256,2816]{0,1:T(8,128)}), f32[256,704]{0,1:T(8,128)}) %reduce-scatter.7.cloned.1.call-update) | async-done | bytes 720912 | tf_op jit(solution)/shard_map/reduce_scatter | solution.py:52
  103.9 2.2 fusion.25
  106.2 12.6 %convert.14 = bf16[2,2816,1024]{2,1,0:T(8,128)(2,1)} convert(f32[2,2816,1024]{2,1,0:T(8,128)} %param.18) | non-fusion elementwise | flops 5767168 | bytes 34603008 | tf_op jit(solution)/shard_map/convert.3
  118.8 6.4 %all-gather.3.cloned.1.call-done = bf16[256,2816]{0,1:T(8,128)(2,1)} async-done(((bf16[256,704]{0,1:T(8,128)(2,1)}), bf16[256,2816]{0,1:T(8,128)(2,1)}) %all-gather.3.cloned.1.call-update) | async-done | bytes 1441808 | tf_op jit(solution)/shard_map/all_gather | solution.py:66
  125.2 5.8 %fusion.3 = f32[256,1024]{1,0:T(8,128)} fusion(bf16[256,2816]{0,1:T(8,128)(2,1)} %all-gather.3.cloned.1.call-done, bf16[2,2816,1024]{2,1,0:T(8,128)(2,1)} %convert.14), kind=kOutput, calls=%fused_computation.7 | convolution fusion | flops 1476395008 | bytes 8257536 | tf_op jit(solution)/shard_map/dot_general | solution.py:67
  131.0 52.0 %all-reduce.7.cloned.1.call-done = f32[256,1024]{1,0:T(8,128)} async-done(((f32[256,1024]{1,0:T(8,128)}), f32[256,1024]{1,0:T(8,128)}) %all-reduce.7.cloned.1.call-update) | async-done | bytes 1048592 | tf_op jit(solution)/shard_map/psum | solution.py:70
  184.5 6.6 %fusion.2 = f32[256,2816]{0,1:T(8,128)} fusion(bf16[2,1024,2816]{2,1,0:T(8,128)(2,1)} %copy-done.1, bf16[256,1024]{1,0:T(8,128)(2,1)S(1)} %get-tuple-element.20, f32[1024]{0:T(1024)S(1)} %bitcast.40), kind=kOutput, calls=%fused_computation.5 | convolution fusion | flops 1477181440 | bytes 9179136 | tf_op jit(solution)/shard_map/dot_general | solution.py:44
  191.4 6.6 %fusion.1 = f32[256,2816]{0,1:T(8,128)} fusion(bf16[2,1024,2816]{2,1,0:T(8,128)(2,1)} %copy-done, bf16[256,1024]{1,0:T(8,128)(2,1)S(1)} %get-tuple-element.20, f32[1024]{0:T(1024)S(1)} %bitcast.41), kind=kOutput, calls=%fused_computation.3 | convolution fusion | flops 1477181440 | bytes 9179136 | tf_op jit(solution)/shard_map/dot_general | solution.py:47
  198.3 6.8 %psum.37 = f32[256,1]{0,1:T(1,128)S(1)} all-reduce(f32[256,1]{0,1:T(1,128)S(1)} %bitcast.34), channel_id=1, replica_groups=mesh['grp'=2,'ra'=4,'cb'=4] {'cb'}, use_global_device_ids=true, to_apply=%region_6.7 | all-reduce | flops 256 | bytes 2048 | tf_op jit(solution)/shard_map/psum | solution.py:21
  205.2 21.6 %reduce-scatter.9.cloned.1.call-done = f32[256,704]{0,1:T(8,128)} async-done(((f32[256,2816]{0,1:T(8,128)}), f32[256,704]{0,1:T(8,128)}) %reduce-scatter.9.cloned.1.call-update) | async-done | bytes 720912 | tf_op jit(solution)/shard_map/reduce_scatter | solution.py:51
  226.8 38.6 %reduce-scatter.11.cloned.1.call-done = f32[256,704]{0,1:T(8,128)} async-done(((f32[256,2816]{0,1:T(8,128)}), f32[256,704]{0,1:T(8,128)}) %reduce-scatter.11.cloned.1.call-update) | async-done | bytes 720912 | tf_op jit(solution)/shard_map/reduce_scatter | solution.py:52
  267.0 2.2 fusion.34
  269.3 19.0 %all-gather.5.cloned.1.call-done = bf16[256,2816]{0,1:T(8,128)(2,1)} async-done(((bf16[256,704]{0,1:T(8,128)(2,1)}), bf16[256,2816]{0,1:T(8,128)(2,1)}) %all-gather.5.cloned.1.call-update) | async-done | bytes 1441808 | tf_op jit(solution)/shard_map/all_gather | solution.py:66
  288.3 5.7 %fusion = f32[256,1024]{1,0:T(8,128)} fusion(bf16[256,2816]{0,1:T(8,128)(2,1)} %all-gather.5.cloned.1.call-done, bf16[2,2816,1024]{2,1,0:T(8,128)(2,1)} %convert.14), kind=kOutput, calls=%fused_computation.1 | convolution fusion | flops 1476395008 | bytes 8257536 | tf_op jit(solution)/shard_map/dot_general | solution.py:67
  294.0 52.1 %all-reduce.9.cloned.1.call-done = f32[256,1024]{1,0:T(8,128)} async-done(((f32[256,1024]{1,0:T(8,128)}), f32[256,1024]{1,0:T(8,128)}) %all-reduce.9.cloned.1.call-update) | async-done | bytes 1048592 | tf_op jit(solution)/shard_map/psum | solution.py:70
  347.6 6.8 %psum.39 = f32[256,1]{0,1:T(1,128)S(1)} all-reduce(f32[256,1]{0,1:T(1,128)S(1)} %bitcast.37), channel_id=1, replica_groups=mesh['grp'=2,'ra'=4,'cb'=4] {'cb'}, use_global_device_ids=true, to_apply=%region_11.12 | all-reduce | flops 256 | bytes 2048 | tf_op jit(solution)/shard_map/psum | solution.py:21
  (49 shorter events, 9.5 us)
Async XLA Ops:
  6.5 57.0 %reduce-scatter.5.cloned.1.call-start = ((), (), s32[]{:S(2)}) async-start(), calls=%async_computation.4 | async-start | bytes 3604480 | tf_op jit(solution)/shard_map/reduce_scatter | solution.py:51
  7.4 12.8 %copy-start.2 = (bf16[256,1024]{1,0:T(8,128)(2,1)S(1)}, bf16[256,1024]{1,0:T(8,128)(2,1)}, u32[]{:S(2)}) copy-start(bf16[256,1024]{1,0:T(8,128)(2,1)} %param.10) | copy-start | bytes 1572868
  16.0 4.2 %copy-start.1 = (bf16[2,1024,2816]{2,1,0:T(8,128)(2,1)}, bf16[2,1024,2816]{2,1,0:T(8,128)(2,1)S(1)}, u32[]{:S(2)}) copy-start(bf16[2,1024,2816]{2,1,0:T(8,128)(2,1)S(1)} %convert.12) | copy-start | bytes 34603012
  24.3 78.0 %reduce-scatter.7.cloned.1.call-start = ((), (), s32[]{:S(2)}) async-start(), calls=%async_computation.5 | async-start | bytes 3604480 | tf_op jit(solution)/shard_map/reduce_scatter | solution.py:52
  32.9 4.8 %copy-start = (bf16[2,1024,2816]{2,1,0:T(8,128)(2,1)}, bf16[2,1024,2816]{2,1,0:T(8,128)(2,1)S(1)}, u32[]{:S(2)}) copy-start(bf16[2,1024,2816]{2,1,0:T(8,128)(2,1)S(1)} %convert.13) | copy-start | bytes 34603012
  37.7 4.1 %copy-start.5 = (f32[2,2816]{1,0:T(2,128)S(1)}, f32[2,2816]{1,0:T(2,128)}, u32[]{:S(2)}) copy-start(f32[2,2816]{1,0:T(2,128)} %param.14) | copy-start | bytes 67588
  37.7 4.1 %copy-start.6 = (f32[2,2816]{1,0:T(2,128)S(1)}, f32[2,2816]{1,0:T(2,128)}, u32[]{:S(2)}) copy-start(f32[2,2816]{1,0:T(2,128)} %param.15) | copy-start | bytes 67588
  37.8 13.5 %copy-start.3 = (f32[2,3,2816]{2,0,1:T(2,128)S(1)}, f32[2,3,2816]{2,0,1:T(2,128)}, u32[]{:S(2)}) copy-start(f32[2,3,2816]{2,0,1:T(2,128)} %param.16) | copy-start | bytes 202756
  37.8 13.5 %copy-start.4 = (f32[2,3,2816]{2,0,1:T(2,128)S(1)}, f32[2,3,2816]{2,0,1:T(2,128)}, u32[]{:S(2)}) copy-start(f32[2,3,2816]{2,0,1:T(2,128)} %param.17) | copy-start | bytes 202756
  41.8 83.4 %all-gather.3.cloned.1.call-start = ((), (), s32[]{:S(2)}) async-start(), calls=%async_computation.6 | async-start | bytes 1802240 | tf_op jit(solution)/shard_map/all_gather | solution.py:66
  106.1 76.9 %all-reduce.7.cloned.1.call-start = ((), (), s32[]{:S(2)}) async-start(), calls=%async_computation.7 | async-start | bytes 2097152 | tf_op jit(solution)/shard_map/psum | solution.py:70
  118.8 12.2 %copy-start.7 = (f32[2,1024]{1,0:T(2,128)S(1)}, f32[2,1024]{1,0:T(2,128)}, u32[]{:S(2)}) copy-start(f32[2,1024]{1,0:T(2,128)} %param.19) | copy-start | bytes 24580
  130.9 95.8 %reduce-scatter.9.cloned.1.call-start = ((), (), s32[]{:S(2)}) async-start(), calls=%async_computation.8 | async-start | bytes 3604480 | tf_op jit(solution)/shard_map/reduce_scatter | solution.py:51
  191.2 74.2 %reduce-scatter.11.cloned.1.call-start = ((), (), s32[]{:S(2)}) async-start(), calls=%async_computation.9 | async-start | bytes 3604480 | tf_op jit(solution)/shard_map/reduce_scatter | solution.py:52
  198.1 90.2 %all-gather.5.cloned.1.call-start = ((), (), s32[]{:S(2)}) async-start(), calls=%async_computation.10 | async-start | bytes 1802240 | tf_op jit(solution)/shard_map/all_gather | solution.py:66
  269.2 76.9 %all-reduce.9.cloned.1.call-start = ((), (), s32[]{:S(2)}) async-start(), calls=%async_computation.11 | async-start | bytes 2097152 | tf_op jit(solution)/shard_map/psum | solution.py:70
Sparse Core Ops, SparseCore 0:
  24.4 39.0 reduce-scatter.4
  66.1 36.1 reduce-scatter.6
  106.2 18.8 all-gather.2
  131.1 51.8 all-reduce.6
  191.3 35.4 reduce-scatter.8
  229.2 36.1 reduce-scatter.10
  269.3 18.8 all-gather.4
  294.1 51.8 all-reduce.8
where the time goes:
time: 363 us; the launch traced here: 362 us
  waiting for transfers between devices  241 us (66%)
  other arithmetic  41.6 us (11%)
  matrix products  32.8 us (9%)
  blocking collectives  22.7 us (6%)
  between operations  13.7 us (4%)
  local copies, waits for them, and re-layouts  10.5 us (3%)
    psum x2, waiting for transfers between devices, on_device(): down_total = lax.psum(partial_value, 'ra')  104 us
    reduce_scatter x2, waiting for transfers between devices, on_device(): lax.psum_scatter(value_part, 'cb', scatter_dimension=1, tiled=True)  77.4 us
    reduce_scatter x2, waiting for transfers between devices, on_device(): lax.psum_scatter(gate_part, 'cb', scatter_dimension=1, tiled=True)  33.6 us
    another operation x3, other arithmetic  29.8 us
    all_gather x2, waiting for transfers between devices, on_device(): hidden = lax.all_gather(hidden, 'cb', axis=1, tiled=True)  25.4 us
    psum x3, blocking collectives, row_inverse(): lax.psum(jnp.sum(state_wide * state_wide, axis=1, keepdims=True), 'cb')  22.7 us
    dot_general x2, matrix products, on_device(): jnp.dot(hidden, down_weight[layer_idx].astype(jnp.bfloat16), preferred_el...  11.5 us
    dot_general x2, matrix products, on_device(): jnp.dot(scaled, gate_weight[layer_idx].astype(jnp.bfloat16), preferred_el...  10.7 us
  transfers between devices with their start and end apart: 8, of which 8 were waited for; matrix products, arithmetic and copies ran while one was open for 9% of the time, Pallas kernels for 0%

commit v1 on v0

--- a/solution.py
+++ b/solution.py
@@ -67,7 +67,8 @@
         partial_value = jnp.dot(
             hidden, down_weight[layer_idx].astype(jnp.bfloat16), preferred_element_type=jnp.float32
         )
-        down_total = lax.psum(partial_value, "ra")
+        shards = lax.all_gather(partial_value, "ra")
+        down_total = jnp.sum(shards, axis=0)
         current = (residual_weight * state_wide + down_scale[layer_idx] * down_total).astype(
             jnp.bfloat16
         )

time: 363 us -> 422 us (1.16)
  waiting for transfers between devices: 241 us -> 298 us
    all_gather x0 -> x2, waiting for transfers between devices: none -> 162 us  [on_device(): shards = lax.all_gather(partial_value, 'ra')]
    psum x2 -> x0, waiting for transfers between devices: 104 us -> none  [on_device(): down_total = lax.psum(partial_value, 'ra')]
    reduce_sum x0 -> x2, other arithmetic: none -> 5.44 us  [on_device(): down_total = jnp.sum(shards, axis=0)]
  transfers between devices with their start and end apart: 8 -> 8, of which waited for: 8 -> 8; matrix products, arithmetic and copies ran while one was open for 9% -> 8% of each run, Pallas kernels for 0% -> 0%
where the time goes in v1:
time: 422 us
  waiting for transfers between devices  298 us (71%)
  other arithmetic  44.6 us (11%)
  matrix products  32.8 us (8%)
  blocking collectives  21.9 us (5%)
  between operations  13.7 us (3%)
  local copies, waits for them, and re-layouts  10.5 us (2%)
    all_gather x2, waiting for transfers between devices, on_device(): shards = lax.all_gather(partial_value, 'ra')  162 us
    reduce_scatter x2, waiting for transfers between devices, on_device(): lax.psum_scatter(value_part, 'cb', scatter_dimension=1, tiled=True)  77.4 us
    reduce_scatter x2, waiting for transfers between devices, on_device(): lax.psum_scatter(gate_part, 'cb', scatter_dimension=1, tiled=True)  33.5 us
    another operation x3, other arithmetic  29.8 us
    all_gather x2, waiting for transfers between devices, on_device(): hidden = lax.all_gather(hidden, 'cb', axis=1, tiled=True)  25.4 us
    psum x3, blocking collectives, row_inverse(): lax.psum(jnp.sum(state_wide * state_wide, axis=1, keepdims=True), 'cb')  21.9 us
    dot_general x2, matrix products, on_device(): jnp.dot(hidden, down_weight[layer_idx].astype(jnp.bfloat16), preferred_el...  11.5 us
    dot_general x2, matrix products, on_device(): jnp.dot(scaled, gate_weight[layer_idx].astype(jnp.bfloat16), preferred_el...  10.7 us
  transfers between devices with their start and end apart: 8, of which 8 were waited for; matrix products, arithmetic and copies ran while one was open for 8% of the time, Pallas kernels for 0%

profile of v1, /device:TPU:0, one launch (start us, length us, event | category | flops | bytes accessed | tf_op | source)
XLA Modules:
  0.0 421.8 jit_solution(424893775356549077)
XLA Ops:
  7.4 8.6 %convert.12 = bf16[2,1024,2816]{2,1,0:T(8,128)(2,1)S(1)} convert(f32[2,1024,2816]{2,1,0:T(8,128)} %param.12) | non-fusion elementwise | flops 5767168 | bytes 34603008 | tf_op jit(solution)/shard_map/convert.5
  16.0 4.2 copy-done.1
  20.2 4.1 fusion.5
  24.4 8.6 %convert.13 = bf16[2,1024,2816]{2,1,0:T(8,128)(2,1)S(1)} convert(f32[2,1024,2816]{2,1,0:T(8,128)} %param.13) | non-fusion elementwise | flops 5767168 | bytes 34603008 | tf_op jit(solution)/shard_map/convert.4
  32.9 4.8 %copy-done = bf16[2,1024,2816]{2,1,0:T(8,128)(2,1)} copy-done((bf16[2,1024,2816]{2,1,0:T(8,128)(2,1)}, bf16[2,1024,2816]{2,1,0:T(8,128)(2,1)S(1)}, u32[]{:S(2)}) %copy-start) | copy-done | bytes 11534360
  37.8 4.0 fusion.4
  42.2 9.0 %psum.21 = f32[256,1]{0,1:T(1,128)S(1)} all-reduce(f32[256,1]{0,1:T(1,128)S(1)} %bitcast.43), channel_id=1, replica_groups=mesh['grp'=2,'ra'=4,'cb'=4] {'cb'}, use_global_device_ids=true, to_apply=%region_1.0 | all-reduce | flops 256 | bytes 2048 | tf_op jit(solution)/shard_map/psum | solution.py:21
  51.5 12.1 %reduce-scatter.5.cloned.1.call-done = f32[256,704]{0,1:T(8,128)} async-done(((f32[256,2816]{0,1:T(8,128)}), f32[256,704]{0,1:T(8,128)}) %reduce-scatter.5.cloned.1.call-update) | async-done | bytes 720912 | tf_op jit(solution)/shard_map/reduce_scatter | solution.py:51
  63.5 38.8 %reduce-scatter.7.cloned.1.call-done = f32[256,704]{0,1:T(8,128)} async-done(((f32[256,2816]{0,1:T(8,128)}), f32[256,704]{0,1:T(8,128)}) %reduce-scatter.7.cloned.1.call-update) | async-done | bytes 720912 | tf_op jit(solution)/shard_map/reduce_scatter | solution.py:52
  106.2 12.6 %convert.14 = bf16[2,2816,1024]{2,1,0:T(8,128)(2,1)} convert(f32[2,2816,1024]{2,1,0:T(8,128)} %param.18) | non-fusion elementwise | flops 5767168 | bytes 34603008 | tf_op jit(solution)/shard_map/convert.3
  118.8 6.4 %all-gather.7.cloned.1.call-done = bf16[256,2816]{0,1:T(8,128)(2,1)} async-done(((bf16[256,704]{0,1:T(8,128)(2,1)}), bf16[256,2816]{0,1:T(8,128)(2,1)}) %all-gather.7.cloned.1.call-update) | async-done | bytes 1441808 | tf_op jit(solution)/shard_map/all_gather | solution.py:66
  125.2 5.7 %fusion.3 = f32[256,1024]{1,0:T(8,128)} fusion(bf16[256,2816]{0,1:T(8,128)(2,1)} %all-gather.7.cloned.1.call-done, bf16[2,2816,1024]{2,1,0:T(8,128)(2,1)} %convert.14), kind=kOutput, calls=%fused_computation.7 | convolution fusion | flops 1476395008 | bytes 8257536 | tf_op jit(solution)/shard_map/dot_general | solution.py:67
  131.2 80.6 %all-gather.11.cloned.1.call-done = f32[1024,1024]{1,0:T(8,128)} async-done(((f32[256,1024]{1,0:T(8,128)}), f32[1024,1024]{1,0:T(8,128)}) %all-gather.11.cloned.1.call-update) | async-done | bytes 4194320 | tf_op jit(solution)/shard_map/all_gather | solution.py:70
  211.8 2.7 reduce_sum.46
  214.8 6.6 %fusion.2 = f32[256,2816]{0,1:T(8,128)} fusion(bf16[2,1024,2816]{2,1,0:T(8,128)(2,1)} %copy-done.1, bf16[256,1024]{1,0:T(8,128)(2,1)S(1)} %get-tuple-element.20, f32[1024]{0:T(1024)S(1)} %bitcast.44), kind=kOutput, calls=%fused_computation.5 | convolution fusion | flops 1477181440 | bytes 9179136 | tf_op jit(solution)/shard_map/dot_general | solution.py:44
  221.5 6.6 %fusion.1 = f32[256,2816]{0,1:T(8,128)} fusion(bf16[2,1024,2816]{2,1,0:T(8,128)(2,1)} %copy-done, bf16[256,1024]{1,0:T(8,128)(2,1)S(1)} %get-tuple-element.20, f32[1024]{0:T(1024)S(1)} %bitcast.45), kind=kOutput, calls=%fused_computation.3 | convolution fusion | flops 1477181440 | bytes 9179136 | tf_op jit(solution)/shard_map/dot_general | solution.py:47
  228.5 6.4 %psum.22 = f32[256,1]{0,1:T(1,128)S(1)} all-reduce(f32[256,1]{0,1:T(1,128)S(1)} %bitcast.38), channel_id=1, replica_groups=mesh['grp'=2,'ra'=4,'cb'=4] {'cb'}, use_global_device_ids=true, to_apply=%region_6.7 | all-reduce | flops 256 | bytes 2048 | tf_op jit(solution)/shard_map/psum | solution.py:21
  234.9 21.4 %reduce-scatter.9.cloned.1.call-done = f32[256,704]{0,1:T(8,128)} async-done(((f32[256,2816]{0,1:T(8,128)}), f32[256,704]{0,1:T(8,128)}) %reduce-scatter.9.cloned.1.call-update) | async-done | bytes 720912 | tf_op jit(solution)/shard_map/reduce_scatter | solution.py:51
  256.3 38.6 %reduce-scatter.11.cloned.1.call-done = f32[256,704]{0,1:T(8,128)} async-done(((f32[256,2816]{0,1:T(8,128)}), f32[256,704]{0,1:T(8,128)}) %reduce-scatter.11.cloned.1.call-update) | async-done | bytes 720912 | tf_op jit(solution)/shard_map/reduce_scatter | solution.py:52
  298.8 19.0 %all-gather.9.cloned.1.call-done = bf16[256,2816]{0,1:T(8,128)(2,1)} async-done(((bf16[256,704]{0,1:T(8,128)(2,1)}), bf16[256,2816]{0,1:T(8,128)(2,1)}) %all-gather.9.cloned.1.call-update) | async-done | bytes 1441808 | tf_op jit(solution)/shard_map/all_gather | solution.py:66
  317.8 5.7 %fusion = f32[256,1024]{1,0:T(8,128)} fusion(bf16[256,2816]{0,1:T(8,128)(2,1)} %all-gather.9.cloned.1.call-done, bf16[2,2816,1024]{2,1,0:T(8,128)(2,1)} %convert.14), kind=kOutput, calls=%fused_computation.1 | convolution fusion | flops 1476395008 | bytes 8257536 | tf_op jit(solution)/shard_map/dot_general | solution.py:67
  323.6 80.9 %all-gather.13.cloned.1.call-done = f32[1024,1024]{1,0:T(8,128)} async-done(((f32[256,1024]{1,0:T(8,128)}), f32[1024,1024]{1,0:T(8,128)}) %all-gather.13.cloned.1.call-update) | async-done | bytes 4194320 | tf_op jit(solution)/shard_map/all_gather | solution.py:70
  404.5 2.7 reduce_sum.48
  407.5 6.4 %psum.23 = f32[256,1]{0,1:T(1,128)S(1)} all-reduce(f32[256,1]{0,1:T(1,128)S(1)} %bitcast.41), channel_id=1, replica_groups=mesh['grp'=2,'ra'=4,'cb'=4] {'cb'}, use_global_device_ids=true, to_apply=%region_11.12 | all-reduce | flops 256 | bytes 2048 | tf_op jit(solution)/shard_map/psum | solution.py:21
  (51 shorter events, 11.4 us)
Async XLA Ops:
  6.5 57.0 %reduce-scatter.5.cloned.1.call-start = ((), (), s32[]{:S(2)}) async-start(), calls=%async_computation.4 | async-start | bytes 3604480 | tf_op jit(solution)/shard_map/reduce_scatter | solution.py:51
  7.4 12.8 %copy-start.2 = (bf16[256,1024]{1,0:T(8,128)(2,1)S(1)}, bf16[256,1024]{1,0:T(8,128)(2,1)}, u32[]{:S(2)}) copy-start(bf16[256,1024]{1,0:T(8,128)(2,1)} %param.10) | copy-start | bytes 1572868
  16.0 4.2 copy-start.1
  24.3 78.0 %reduce-scatter.7.cloned.1.call-start = ((), (), s32[]{:S(2)}) async-start(), calls=%async_computation.5 | async-start | bytes 3604480 | tf_op jit(solution)/shard_map/reduce_scatter | solution.py:52
  32.9 4.8 %copy-start = (bf16[2,1024,2816]{2,1,0:T(8,128)(2,1)}, bf16[2,1024,2816]{2,1,0:T(8,128)(2,1)S(1)}, u32[]{:S(2)}) copy-start(bf16[2,1024,2816]{2,1,0:T(8,128)(2,1)S(1)} %convert.13) | copy-start | bytes 34603012
  37.7 4.1 copy-start.5
  37.7 4.1 copy-start.6
  37.8 13.5 %copy-start.3 = (f32[2,3,2816]{2,0,1:T(2,128)S(1)}, f32[2,3,2816]{2,0,1:T(2,128)}, u32[]{:S(2)}) copy-start(f32[2,3,2816]{2,0,1:T(2,128)} %param.16) | copy-start | bytes 202756
  37.8 13.5 %copy-start.4 = (f32[2,3,2816]{2,0,1:T(2,128)S(1)}, f32[2,3,2816]{2,0,1:T(2,128)}, u32[]{:S(2)}) copy-start(f32[2,3,2816]{2,0,1:T(2,128)} %param.17) | copy-start | bytes 202756
  41.8 83.4 %all-gather.7.cloned.1.call-start = ((), (), s32[]{:S(2)}) async-start(), calls=%async_computation.6 | async-start | bytes 1802240 | tf_op jit(solution)/shard_map/all_gather | solution.py:66
  106.1 105.7 %all-gather.11.cloned.1.call-start = ((), (), s32[]{:S(2)}) async-start(), calls=%async_computation.10 | async-start | bytes 5242880 | tf_op jit(solution)/shard_map/all_gather | solution.py:70
  118.8 12.3 %copy-start.7 = (f32[2,1024]{1,0:T(2,128)S(1)}, f32[2,1024]{1,0:T(2,128)}, u32[]{:S(2)}) copy-start(f32[2,1024]{1,0:T(2,128)} %param.19) | copy-start | bytes 24580
  130.9 125.4 %reduce-scatter.9.cloned.1.call-start = ((), (), s32[]{:S(2)}) async-start(), calls=%async_computation.7 | async-start | bytes 3604480 | tf_op jit(solution)/shard_map/reduce_scatter | solution.py:51
  221.5 73.5 %reduce-scatter.11.cloned.1.call-start = ((), (), s32[]{:S(2)}) async-start(), calls=%async_computation.8 | async-start | bytes 3604480 | tf_op jit(solution)/shard_map/reduce_scatter | solution.py:52
  228.2 89.6 %all-gather.9.cloned.1.call-start = ((), (), s32[]{:S(2)}) async-start(), calls=%async_computation.9 | async-start | bytes 1802240 | tf_op jit(solution)/shard_map/all_gather | solution.py:66
  298.8 105.7 %all-gather.13.cloned.1.call-start = ((), (), s32[]{:S(2)}) async-start(), calls=%async_computation.11 | async-start | bytes 5242880 | tf_op jit(solution)/shard_map/all_gather | solution.py:70
Sparse Core Ops, SparseCore 0:
  24.4 39.0 reduce-scatter.4
  66.1 36.1 reduce-scatter.6
  106.2 18.8 all-gather.6
  131.0 80.7 all-gather.10
  221.6 34.6 reduce-scatter.8
  258.7 36.1 reduce-scatter.10
  298.9 18.8 all-gather.8
  323.7 80.7 all-gather.12
